TPU v7x, 32 devices: a whole 2x2x4 slice. The times are simulated.
32 devices in a mesh: ep: 8 (over z, x), tp: 4 (over y, core).
Axes of the slice: x: 2, y: 2, z: 4, core: 2. Of those that a mesh axis runs over, the one named last changes fastest.
Arguments:
- mixer_rows: bfloat16 [1024, 2048], P('ep'), may hold values from -40 to 40
- mixer_gain: float32 [2048], replicated, may hold values from 0.1 to 1.9
- inner_weight: bfloat16 [2048, 1024], P(None, 'tp'), may hold values from -0.125 to 0.125
- gate_in_weight: bfloat16 [2048, 1024], P(None, 'tp'), may hold values from -0.125 to 0.125
- gate_out_weight: bfloat16 [2048, 1024], P(None, 'tp'), may hold values from -0.125 to 0.125
- conv_taps: float32 [3, 1024], P(None, 'tp'), may hold values from -3.5 to 3.5
- mixer_out_weight: bfloat16 [1024, 2048], P('tp'), may hold values from -0.1875 to 0.1875
- routed_rows: bfloat16 [2048, 2048], P('ep'), may hold values from -40 to 40
- routed_gain: float32 [2048], replicated, may hold values from 0.1 to 1.9
- route_ids: int32 [2048, 2], P('ep'), may hold values from 0 to 7, all different within a row; in each aligned block of 256 rows (0 to 255, 256 to 511, ...) at most 128 rows name the same one
- route_weights: float32 [2048, 2], P('ep'), may hold values from 0.25 to 1
- expert_gate: bfloat16 [8, 2048, 2048], P('ep', None, 'tp'), may hold values from -0.125 to 0.125
- expert_up: bfloat16 [8, 2048, 2048], P('ep', None, 'tp'), may hold values from -0.125 to 0.125
- expert_down: bfloat16 [8, 2048, 2048], P('ep', 'tp'), may hold values from -0.125 to 0.125
Outputs:
- mixer_output: bfloat16 [1024, 2048], P('ep')
- routed_output: bfloat16 [2048, 2048], P('ep')
Inputs may be any that keep to these rules, and one draw needn't show every extreme that they name: `route_ids`: within each aligned block of 256 tokens, no expert is named by more than 128 choices, a bound that some block reaches; a token's 2 experts differ.
All inputs are finite; a program needn't handle non-finite values.
Results may differ from a plain program's by a relative error of at most 0.019.
Values may be sent and summed in bfloat16 or wider, within the bound.
A program may use at most 64 MiB of HBM per device.

v0:
```python
import jax
import jax.numpy as jnp
from jax import lax
from jax.experimental import pallas as pl
from jax.experimental.pallas import tpu as pltpu
from jax.sharding import PartitionSpec as P

F32, BF16, I32 = jnp.float32, jnp.bfloat16, jnp.int32
CORES = 2


def rms(values):
    return lax.rsqrt(jnp.mean(values * values, axis=-1, keepdims=True) + 1e-06)


def dot(a, b):
    return jnp.dot(a, b, preferred_element_type=F32)


def make_kernel(experts, groups, tok, picks, width, cap, steps, per, mrows, taps_n, chan):
    high = groups // CORES
    whole = 1
    half = steps // 2
    order = list(range(half, steps)) + list(range(half - 1, -1, -1))
    slab = width // groups
    rows = per * cap

    def kernel(
        mixer_rows, mixer_gain, inner_h, gate_in_h, gate_out_h, taps, mixer_out_h,
        routed_rows, routed_gain, ids, weights, gate_h, up_h, down_h,
        out_m, out_r,
        w_inner, w_gin, w_gout, w_mout, w_gate, w_up, w_down,
        disp, slots, part, r1, s2, r2, t3, ret,
        rim, rim_in, m_part, m_r1, m_s2, m_r2,
        w_sem, own_sem,
        d1_s, d1_r, y_s, y_r, b_s, b_r, e_s, e_r, g_s, g_r, ret_s, ret_r,
        rim_s, rim_r, ay_s, ay_r, ab_s, ab_r,
    ):
        me = lax.axis_index("ep")
        t = lax.axis_index("tp")
        yy, cc = t // CORES, t % CORES
        mate = yy * CORES + (1 - cc)
        my_chunk, my_j = me // per, me % per
        sent = []

        def send(src, dst, ssem, rsem, where):
            copy = pltpu.make_async_remote_copy(
                src_ref=src, dst_ref=dst, send_sem=ssem, recv_sem=rsem,
                device_id=where, device_id_type=pl.DeviceIdType.MESH,
            )
            copy.start()
            sent.append(copy)

        def arrive(dst, ssem, rsem):
            pltpu.make_async_remote_copy(
                src_ref=dst, dst_ref=dst, send_sem=ssem, recv_sem=rsem,
                device_id={"tp": mate}, device_id_type=pl.DeviceIdType.MESH,
            ).wait_recv()

        def up_to(dy):
            return lax.rem(yy + dy, high)

        def down_to(dy):
            return lax.rem(yy + high - dy, high)

        loads = []
        for place, (src, dst) in enumerate(
            (
                (inner_h, w_inner), (gate_in_h, w_gin), (gate_out_h, w_gout), (mixer_out_h, w_mout),
                (gate_h, w_gate), (up_h, w_up), (down_h, w_down),
            )
        ):
            copy = pltpu.make_async_copy(src, dst, w_sem.at[place])
            copy.start()
            loads.append(copy)

        barrier = pltpu.get_barrier_semaphore()
        for d in range(1, experts):
            pl.semaphore_signal(
                barrier, inc=1, device_id={"ep": lax.rem(me + d, experts)},
                device_id_type=pl.DeviceIdType.MESH,
            )
        for dy in range(1, high):
            pl.semaphore_signal(
                barrier, inc=1, device_id={"tp": up_to(dy) * CORES + cc},
                device_id_type=pl.DeviceIdType.MESH,
            )
        pl.semaphore_signal(
            barrier, inc=1, device_id={"tp": mate}, device_id_type=pl.DeviceIdType.MESH
        )

        row = lax.broadcasted_iota(I32, (128, tok), 0)
        hits = [row == ids[k : k + 1, :] for k in range(picks)]
        named = sum(h.astype(F32) for h in hits)
        before = (
            lax.broadcasted_iota(I32, (tok, tok), 0) < lax.broadcasted_iota(I32, (tok, tok), 1)
        ).astype(F32).astype(BF16)
        earlier = dot(named.astype(BF16), before)
        slot_row = lax.broadcasted_iota(I32, (experts * cap, tok), 0)
        pick_map = jnp.zeros((experts * cap, tok), F32)
        sum_map = jnp.zeros((experts * cap, tok), F32)
        for k in range(picks):
            rank = jnp.sum(jnp.where(hits[k], earlier, 0.0), axis=0, keepdims=True).astype(I32)
            at = slot_row == (ids[k : k + 1, :] * cap + rank)
            pick_map = pick_map + jnp.where(at, 1.0, 0.0)
            sum_map = sum_map + jnp.where(at, weights[k : k + 1, :], 0.0)
        pick_map, sum_map = pick_map.astype(BF16), sum_map.astype(BF16)

        my_cols = pl.ds(pl.multiple_of(t * slab, slab), slab)
        scale = rms(routed_rows[...].astype(F32))
        for y in range(high):
            cols = pl.ds(pl.multiple_of((y * CORES + cc) * slab, slab), slab)
            normed = ((routed_rows[:, cols].astype(F32) * scale) * routed_gain[:, cols]).astype(BF16)
            disp[y] = dot(pick_map, normed).astype(BF16).reshape(experts, cap, slab)
        pl.semaphore_wait(barrier, experts - 1 + high - 1 + 1)

        def others(i):
            return [j if i else lax.rem(my_j + j + 1, per) for j in range(per if i else per - 1)]

        def partner(i):
            chunk = my_chunk
            for bit in (1 << n for n in range(i.bit_length())):
                if i & bit:
                    chunk = chunk + bit - 2 * bit * lax.rem(chunk // bit, 2)
            return chunk

        def slabs(i):
            return range(high if i < whole else 1)

        for i in order:
            for jj in others(i):
                dest = partner(i) * per + jj
                for dy in slabs(i):
                    y = down_to(dy)
                    send(
                        disp.at[y, dest], slots.at[y * CORES + cc, i, my_j],
                        d1_s.at[i, jj, dy], d1_r.at[i, my_j, dy], {"ep": dest},
                    )
        own = []
        for y in range(high):
            copy = pltpu.make_async_copy(
                disp.at[y, me], slots.at[y * CORES + cc, 0, my_j], own_sem.at[y]
            )
            copy.start()
            own.append(copy)

        def stage_a(i):
            for jj in others(i):
                for dy in slabs(i):
                    arrive(
                        slots.at[down_to(dy) * CORES + cc, i, jj], d1_s.at[i, jj, dy], d1_r.at[i, jj, dy]
                    )
            if i == 0:
                for copy in own:
                    copy.wait()
            if i >= whole:
                for dy in range(1, high):
                    send(
                        slots.at[t, i], slots.at[t, i], y_s.at[i, dy - 1], y_r.at[i, dy - 1],
                        {"tp": up_to(dy) * CORES + cc},
                    )
            for dy in slabs(i):
                block = slots.at[down_to(dy) * CORES + cc, i]
                send(block, block, b_s.at[i, dy], b_r.at[i, dy], {"tp": mate})

        def stage_b(i):
            if i < whole:
                return
            for dy in range(1, high):
                block = slots.at[down_to(dy) * CORES + cc, i]
                arrive(block, y_s.at[i, dy - 1], y_r.at[i, dy - 1])
                send(block, block, b_s.at[i, dy], b_r.at[i, dy], {"tp": mate})

        def stage_c(i):
            for dy in range(high):
                arrive(
                    slots.at[down_to(dy) * CORES + (1 - cc), i], b_s.at[i, dy], b_r.at[i, dy]
                )
            x = jnp.concatenate([slots[q, i].reshape(rows, slab) for q in range(groups)], axis=1)
            gate, up = dot(x, w_gate[...]), dot(x, w_up[...])
            hidden = (gate / (1.0 + jnp.exp(-gate)) * up).astype(BF16)
            for q in range(groups):
                part[i, q % CORES, q // CORES] = dot(
                    hidden, w_down[:, q * slab : (q + 1) * slab]
                ).astype(BF16)
            send(part.at[i, 1 - cc], r1.at[i], e_s.at[i], e_r.at[i], {"tp": mate})

        def pair_sum(i, part_i, r1_i, s2_i, r2_i):
            arrive(r1_i, e_s.at[i], e_r.at[i])
            for y in range(high):
                s2_i[y] = (part_i[cc, y].astype(F32) + r1_i[y].astype(F32)).astype(BF16)
            for dy in range(1, high):
                send(
                    s2_i.at[up_to(dy)], r2_i.at[dy - 1], g_s.at[i, dy - 1], g_r.at[i, dy - 1],
                    {"tp": up_to(dy) * CORES + cc},
                )

        def chip_sum(i, s2_i, r2_i):
            total = s2_i[yy].astype(F32)
            for dy in range(1, high):
                arrive(r2_i.at[dy - 1], g_s.at[i, dy - 1], g_r.at[i, dy - 1])
                total = total + r2_i[dy - 1].astype(F32)
            return total.astype(BF16)

        def stage_e(i):
            pair_sum(i, part.at[i], r1.at[i], s2.at[i], r2.at[i])

        def stage_g(i):
            t3[i] = chip_sum(i, s2.at[i], r2.at[i]).reshape(per, cap, slab)
            for jj in others(i):
                dest = partner(i) * per + jj
                send(t3.at[i, jj], ret.at[me], ret_s.at[i, jj], ret_r.at[me], {"ep": dest})
            if i == 0:
                ret[me] = t3[0, my_j]

        def spread(which, out, value):
            out[:, my_cols] = value
            window = out.at[:, my_cols]
            for dy in range(1, high):
                send(
                    window, window, ay_s.at[which, dy - 1], ay_r.at[which, dy - 1],
                    {"tp": up_to(dy) * CORES + cc},
                )
            send(window, window, ab_s.at[which, 0], ab_r.at[which, 0], {"tp": mate})

        def window_of(out, group):
            return out.at[:, pl.ds(pl.multiple_of(group * slab, slab), slab)]

        def spread_on(which, out):
            for dy in range(1, high):
                window = window_of(out, down_to(dy) * CORES + cc)
                arrive(window, ay_s.at[which, dy - 1], ay_r.at[which, dy - 1])
                send(window, window, ab_s.at[which, dy], ab_r.at[which, dy], {"tp": mate})

        def spread_end(which, out):
            for dy in range(high):
                arrive(
                    window_of(out, down_to(dy) * CORES + (1 - cc)),
                    ab_s.at[which, dy], ab_r.at[which, dy],
                )

        for copy in loads[:4]:
            copy.wait()
        mixed = mixer_rows[...].astype(F32)
        mixed = ((mixed * rms(mixed)) * mixer_gain[...]).astype(BF16)
        conv_input = (dot(mixed, w_gin[...]) * dot(mixed, w_inner[...])).astype(BF16)
        edge = rim.shape[0]
        rim[...] = conv_input[mrows - edge :]
        send(rim, rim_in, rim_s.at[0], rim_r.at[0], {"ep": lax.rem(me + 1, experts)})
        gate_out = dot(mixed, w_gout[...])
        stage_a(order[0])
        arrive(rim_in, rim_s.at[0], rim_r.at[0])
        first = jnp.where(me == 0, 0.0, rim_in[...].astype(F32))
        extended = jnp.concatenate([first, conv_input.astype(F32)], axis=0)
        conv = jnp.zeros((mrows, chan), F32)
        for k in range(taps_n):
            start = edge - (taps_n - 1) + k
            conv = conv + taps[k : k + 1, :] * extended[start : start + mrows]
        gated = (gate_out * conv).astype(BF16)
        for q in range(groups):
            m_part[q % CORES, q // CORES] = dot(gated, w_mout[:, q * slab : (q + 1) * slab]).astype(BF16)
        send(m_part.at[1 - cc], m_r1, e_s.at[steps], e_r.at[steps], {"tp": mate})

        for copy in loads[4:]:
            copy.wait()
        for s in range(steps):
            stage_b(order[s])
            stage_c(order[s])
            if s + 1 < steps:
                stage_a(order[s + 1])
            if s == 0:
                pair_sum(steps, m_part, m_r1, m_s2, m_r2)
            stage_e(order[s])
            if s == 1:
                spread(0, out_m, chip_sum(steps, m_s2, m_r2))
            if s == 2:
                spread_on(0, out_m)
            if s >= 1:
                stage_g(order[s - 1])
        stage_g(order[steps - 1])

        for d in range(1, experts):
            e = lax.rem(me + d, experts)
            arrive(ret.at[e], ret_s.at[0, 0], ret_r.at[e])
        summed = lax.dot_general(
            sum_map, ret[...].reshape(experts * cap, slab), (((0,), (0,)), ((), ())),
            preferred_element_type=F32,
        )
        spread(1, out_r, summed.astype(BF16))
        spread_on(1, out_r)
        spread_end(0, out_m)
        spread_end(1, out_r)
        for copy in sent:
            copy.wait_send()

    edge = 16 * -(-(taps_n - 1) // 16)
    dma = pltpu.SemaphoreType.DMA
    far = max(1, high - 1)
    v = lambda shape: pltpu.VMEM(shape, BF16)

    def scratch(hid):
        return [
            v((width, chan)), v((width, chan)), v((width, chan)), v((chan, width)),
            v((width, hid)), v((width, hid)), v((hid, width)),
            v((high, experts, cap, slab)), v((groups, steps, per, cap, slab)),
            v((steps, CORES, high, rows, slab)), v((steps, high, rows, slab)),
            v((steps, high, rows, slab)), v((steps, far, rows, slab)),
            v((steps, per, cap, slab)), v((experts, cap, slab)),
            v((edge, chan)), v((edge, chan)),
            v((CORES, high, mrows, slab)), v((high, mrows, slab)), v((high, mrows, slab)),
            v((far, mrows, slab)),
            dma((7,)), dma((high,)),
            dma((steps, per, high)), dma((steps, per, high)), dma((steps, far)), dma((steps, far)),
            dma((steps, high)), dma((steps, high)), dma((steps + 1,)), dma((steps + 1,)),
            dma((steps + 1, far)), dma((steps + 1, far)), dma((steps, per)), dma((experts,)),
            dma((1,)), dma((1,)), dma((2, far)), dma((2, far)), dma((2, high)), dma((2, high)),
        ]

    return kernel, scratch


def on_device(
    mixer_rows, mixer_gain, inner_weight, gate_in_weight, gate_out_weight, conv_taps,
    mixer_out_weight, routed_rows, routed_gain, route_ids, route_weights,
    expert_gate, expert_up, expert_down,
):
    experts, groups = lax.axis_size("ep"), lax.axis_size("tp")
    tok, picks = route_ids.shape
    width = routed_rows.shape[1]
    cap = 2 * tok * picks // experts
    per = max(1, min(experts, tok // cap))
    steps = experts // per
    mrows = mixer_rows.shape[0]
    taps_n, chan = conv_taps.shape
    kernel, scratch = make_kernel(
        experts, groups, tok, picks, width, cap, steps, per, mrows, taps_n, chan
    )
    near, far = pl.BlockSpec(memory_space=pltpu.VMEM), pl.BlockSpec(memory_space=pl.ANY)
    return pl.pallas_call(
        kernel,
        out_shape=(
            jax.ShapeDtypeStruct(mixer_rows.shape, BF16),
            jax.ShapeDtypeStruct(routed_rows.shape, BF16),
        ),
        in_specs=[near, near, far, far, far, near, far, near, near, near, near, far, far, far],
        out_specs=(near, near),
        scratch_shapes=scratch(expert_gate.shape[2]),
        compiler_params=pltpu.CompilerParams(
            collective_id=0, has_side_effects=True, vmem_limit_bytes=60 * 1024 * 1024
        ),
        name="mixer_and_experts",
    )(
        mixer_rows, mixer_gain[None, :], inner_weight, gate_in_weight, gate_out_weight, conv_taps,
        mixer_out_weight, routed_rows, routed_gain[None, :], route_ids.T, route_weights.T,
        expert_gate[0], expert_up[0], expert_down[0],
    )


def solution(mesh):
    return jax.shard_map(
        on_device,
        mesh=mesh,
        in_specs=(
            P("ep", None), P(), P(None, "tp"), P(None, "tp"), P(None, "tp"), P(None, "tp"),
            P("tp", None), P("ep", None), P(), P("ep", None), P("ep", None),
            P("ep", None, "tp"), P("ep", None, "tp"), P("ep", "tp", None),
        ),
        out_specs=(P("ep", None), P("ep", None)),
        check_vma=False,
    )
```

profile of v0, /device:TPU:0, one launch (start us, length us, event | category | flops | bytes accessed | tf_op | source)
XLA Modules:
  0.0 96.9 jit_solution(18305409999321363038)
XLA Ops:
  0.6 92.0 %mixer_and_experts.1 = (bf16[128,2048]{1,0:T(8,128)(2,1)}, bf16[256,2048]{1,0:T(8,128)(2,1)}) custom-call(bf16[128,2048]{1,0:T(8,128)(2,1)} %mixer_rows.1, f32[1,2048]{1,0:T(1,128)} %bitcast.10, bf16[2048,256]{1,0:T(8,128)(2,1)} %inner_h.1, bf16[2048,256]{1,0:T(8,128)(2,1)} %gate_in_h.1, bf16[2048,256]{1,0:T(8,128)(2,1)} %gate_out_h.1, f32[3,256]{1,0:T(4,128)} %taps.1, ...), custom_call_target="tpu_custom_call" | custom-call | tf_op jit(solution)/shard_map/mixer_and_experts/pallas_call | solution.py:339
  92.7 1.9 %copy.18 = bf16[128,2048]{1,0:T(8,128)(2,1)} copy(bf16[128,2048]{1,0:T(8,128)(2,1)} %get-tuple-element.4) | data formatting | bytes 1048576
  94.6 2.3 %copy.19 = bf16[256,2048]{1,0:T(8,128)(2,1)} copy(bf16[256,2048]{1,0:T(8,128)(2,1)} %get-tuple-element.5) | data formatting | bytes 2097152
where the time goes:
time: 97.1 us; the launch traced here: 96.9 us
  Pallas kernels  92 us (95%)
  local copies, waits for them, and re-layouts  4.18 us (4%)
    pallas_call x1, Pallas kernels, on_device(): pl.pallas_call(kernel, out_shape=(jax.ShapeDtypeStruct(mixer_rows.shape,...  92 us
    unnamed x2, local copies, waits for them, and re-layouts  4.18 us

commit v1 on v0

v1 whole, which is shorter than its diff:
```python
import jax
import jax.numpy as jnp
from jax import lax
from jax.experimental import pallas as pl
from jax.experimental.pallas import tpu as pltpu
from jax.sharding import PartitionSpec as P

F32, BF16, I32 = jnp.float32, jnp.bfloat16, jnp.int32
CORES = 2


def rms(values):
    return lax.rsqrt(jnp.mean(values * values, axis=-1, keepdims=True) + 1e-06)


def dot(a, b):
    return jnp.dot(a, b, preferred_element_type=F32)


ORDER = (
    "W", "C00", "E00", "M", "N", "A01", "Aa0", "O", "C01", "E01",
    "Aa1", "Ba0", "Ca0", "Ea0", "A10", "Ab0", "P", "Ba1", "Ca1", "Ea1",
    "G00", "G01", "Ga0", "Ab1", "A11", "Bb0", "Cb0", "Eb0", "Ga1", "C10",
    "E10", "Bb1", "Cb1", "Gb0", "Eb1", "C11", "E11", "Gb1", "G10", "G11",
)
QUEUE = ("01", "20", "30", "21", "31", "10", "11")


def schedule(steps, per, whole):
    if steps == 4 and per == 2 and whole == 2:
        return 2, QUEUE, ORDER
    queue = [str(i) for i in range(steps)]
    order = ["M", "N", "W", "A00", "C00", "O", "E00", "P"]
    for last, i in zip(queue, queue[1:]):
        order += [name + i + "0" for name in ("AC" if int(i) < whole else "ABC") + "E"]
        order.append("G" + last + "0")
    return 1, [i + "0" for i in queue], order + ["G" + queue[-1] + "0"]


def make_kernel(
    experts, groups, tok, picks, width, cap, steps, per, mrows, taps_n, chan, hid, whole, halves, queue, order, pieces
):
    high = groups // CORES
    slab = width // groups
    wide = slab // pieces
    size = per // halves
    rows = size * cap
    edge = 16 * -(-(taps_n - 1) // 16)

    def kernel(
        mixer_h, mixer_gain_h, inner_h, gate_in_h, gate_out_h, taps_h, mixer_out_h,
        routed_h, routed_gain_h, ids_h, weights_h, gate_h, up_h, down_h,
        out_m, out_r,
        mixer_rows, mixer_gain, taps, routed_rows, routed_gain, ids, weights,
        w_inner, w_gin, w_gout, w_mout, w_gate, w_up, w_down,
        disp, slots, part, r1, s2, r2, t3, ret,
        rim, rim_in, m_part, m_r1, m_s2, m_r2,
        w_sem, own_sem,
        d1_s, d1_r, y_s, y_r, b_s, b_r, e_s, e_r, g_s, g_r, ret_s, ret_r,
        rim_s, rim_r, me_s, me_r, mg_s, mg_r, ay_s, ay_r, ab_s, ab_r,
    ):
        me = lax.axis_index("ep")
        t = lax.axis_index("tp")
        yy, cc = t // CORES, t % CORES
        mate = yy * CORES + (1 - cc)
        my_chunk, my_j = me // per, me % per
        sent = []

        def send(src, dst, ssem, rsem, where):
            copy = pltpu.make_async_remote_copy(
                src_ref=src, dst_ref=dst, send_sem=ssem, recv_sem=rsem,
                device_id=where, device_id_type=pl.DeviceIdType.MESH,
            )
            copy.start()
            sent.append(copy)

        def arrive(dst, ssem, rsem):
            pltpu.make_async_remote_copy(
                src_ref=dst, dst_ref=dst, send_sem=ssem, recv_sem=rsem,
                device_id={"tp": mate}, device_id_type=pl.DeviceIdType.MESH,
            ).wait_recv()

        def up_to(dy):
            return lax.rem(yy + dy, high)

        def down_to(dy):
            return lax.rem(yy + high - dy, high)

        barrier = pltpu.get_barrier_semaphore()
        for d in range(1, experts):
            pl.semaphore_signal(
                barrier, inc=1, device_id={"ep": lax.rem(me + d, experts)},
                device_id_type=pl.DeviceIdType.MESH,
            )
        for dy in range(1, high):
            pl.semaphore_signal(
                barrier, inc=1, device_id={"tp": up_to(dy) * CORES + cc},
                device_id_type=pl.DeviceIdType.MESH,
            )
        pl.semaphore_signal(
            barrier, inc=1, device_id={"tp": mate}, device_id_type=pl.DeviceIdType.MESH
        )

        loads = {}
        for place, (name, src, dst) in enumerate(
            (
                ("ids", ids_h, ids), ("weights", weights_h, weights),
                ("mixer", mixer_h, mixer_rows), ("mgain", mixer_gain_h, mixer_gain),
                ("gin", gate_in_h, w_gin), ("inner", inner_h, w_inner),
                ("routed", routed_h, routed_rows), ("rgain", routed_gain_h, routed_gain),
                ("taps", taps_h, taps), ("gout", gate_out_h, w_gout), ("mout", mixer_out_h, w_mout),
                ("gate", gate_h, w_gate), ("up", up_h, w_up), ("down", down_h, w_down),
            )
        ):
            loads[name] = pltpu.make_async_copy(src, dst, w_sem.at[place])
            loads[name].start()

        def loaded(*names):
            for name in names:
                loads[name].wait()

        with jax.named_scope("route"):
            loaded("ids", "weights")
            row = lax.broadcasted_iota(I32, (128, tok), 0)
            hits = [row == ids[k : k + 1, :] for k in range(picks)]
            named = sum(h.astype(F32) for h in hits)
            before = (
                lax.broadcasted_iota(I32, (tok, tok), 0) < lax.broadcasted_iota(I32, (tok, tok), 1)
            ).astype(F32).astype(BF16)
            earlier = dot(named.astype(BF16), before)
            slot_row = lax.broadcasted_iota(I32, (experts * cap, tok), 0)
            pick_map = jnp.zeros((experts * cap, tok), F32)
            sum_map = jnp.zeros((experts * cap, tok), F32)
            for k in range(picks):
                rank = jnp.sum(jnp.where(hits[k], earlier, 0.0), axis=0, keepdims=True).astype(I32)
                at = slot_row == (ids[k : k + 1, :] * cap + rank)
                pick_map = pick_map + jnp.where(at, 1.0, 0.0)
                sum_map = sum_map + jnp.where(at, weights[k : k + 1, :], 0.0)
            pick_map, sum_map = pick_map.astype(BF16), sum_map.astype(BF16)

        my_cols = pl.ds(pl.multiple_of(t * slab, slab), slab)

        with jax.named_scope("mix1"):
            loaded("mixer", "mgain", "gin", "inner")
            mixed = mixer_rows[...].astype(F32)
            mixed = ((mixed * rms(mixed)) * mixer_gain[...]).astype(BF16)
            conv_input = (dot(mixed, w_gin[...]) * dot(mixed, w_inner[...])).astype(BF16)
            rim[...] = conv_input[mrows - edge :]

        def pick(dy, scale):
            y = down_to(dy)
            cols = pl.ds(pl.multiple_of((y * CORES + cc) * slab, slab), slab)
            normed = ((routed_rows[:, cols].astype(F32) * scale) * routed_gain[:, cols]).astype(BF16)
            disp[dy] = dot(pick_map, normed).astype(BF16).reshape(experts, cap, slab)

        with jax.named_scope("pick"):
            loaded("routed", "rgain")
            scale = rms(routed_rows[...].astype(F32))
            pick(0, scale)

        with jax.named_scope("barrier"):
            pl.semaphore_wait(barrier, experts - 1 + high - 1 + 1)
        send(rim, rim_in, rim_s.at[0], rim_r.at[0], {"ep": lax.rem(me + 1, experts)})

        def blocks(h):
            return [lax.rem(my_j + h * size + n, per) for n in range(size)]

        def is_own(i, h, n):
            return i == "0" and h == 0 and n == 0

        outer = 1 - (my_chunk + 1) // 2 % 2
        index = {"a": 2 + outer, "b": 3 - outer}

        def at(i):
            return index[i] if i in index else int(i)

        def far(i):
            return i in index or int(i) >= whole

        def partner(i):
            chunk, other = my_chunk, at(i)
            for bit in (1 << n for n in range((steps - 1).bit_length())):
                chunk = chunk + other // bit % 2 * (bit - 2 * bit * lax.rem(chunk // bit, 2))
            return chunk

        def slabs(i):
            return range(1 if far(i) else high)

        def dispatch(i, h):
            for n, jj in enumerate(blocks(h)):
                if not is_own(i, h, n):
                    dest = partner(i) * per + jj
                    for dy in slabs(i):
                        send(
                            disp.at[dy, dest], slots.at[down_to(dy) * CORES + cc, at(i), my_j],
                            d1_s.at[at(i), jj, dy], d1_r.at[at(i), my_j, dy], {"ep": dest},
                        )

        own = []

        def keep(dy):
            block = slots.at[down_to(dy) * CORES + cc, 0, my_j]
            send(disp.at[dy, me], block, b_s.at[0, dy, my_j], b_r.at[0, dy, my_j], {"tp": mate})
            copy = pltpu.make_async_copy(disp.at[dy, me], block, own_sem.at[dy])
            copy.start()
            own.append(copy)

        with jax.named_scope("dispatch"):
            keep(0)
            for dy in range(1, high):
                pick(dy, scale)
                keep(dy)
            for word in queue:
                dispatch(word[0], int(word[1]))

        def stage_a(i, h):
            k = at(i)
            for n, jj in enumerate(blocks(h)):
                if is_own(i, h, n):
                    continue
                for dy in slabs(i):
                    block = slots.at[down_to(dy) * CORES + cc, k, jj]
                    arrive(block, d1_s.at[k, jj, dy], d1_r.at[k, jj, dy])
                    if far(i):
                        for up in range(1, high):
                            send(
                                block, block, y_s.at[k, up - 1, jj], y_r.at[k, up - 1, jj],
                                {"tp": up_to(up) * CORES + cc},
                            )
                    send(block, block, b_s.at[k, dy, jj], b_r.at[k, dy, jj], {"tp": mate})

        def stage_b(i, h):
            k = at(i)
            for dy in range(1, high):
                for jj in blocks(h):
                    block = slots.at[down_to(dy) * CORES + cc, k, jj]
                    arrive(block, y_s.at[k, dy - 1, jj], y_r.at[k, dy - 1, jj])
                    send(block, block, b_s.at[k, dy, jj], b_r.at[k, dy, jj], {"tp": mate})

        turns = list(range(1, high)) + [0]

        def columns(dy, core):
            return pl.ds(pl.multiple_of((up_to(dy) * CORES + core) * slab, slab), slab)

        def stage_c(i, h):
            k = at(i)
            for dy in range(high):
                for jj in blocks(h):
                    arrive(
                        slots.at[down_to(dy) * CORES + (1 - cc), k, jj],
                        b_s.at[k, dy, jj], b_r.at[k, dy, jj],
                    )
            if is_own(i, h, 0):
                for copy in own:
                    copy.wait()
            x = jnp.concatenate(
                [
                    jnp.concatenate([slots[q, k, jj] for q in range(groups)], axis=1)
                    for jj in blocks(h)
                ],
                axis=0,
            )
            gate, up = dot(x, w_gate[...]), dot(x, w_up[...])
            hidden = (gate / (1.0 + jnp.exp(-gate)) * up).astype(BF16)
            for side, core in ((0, 1 - cc), (1, cc)):
                for dy in turns:
                    value = dot(hidden, w_down[:, columns(dy, core)]).astype(BF16)
                    for p in range(pieces):
                        part[k, h, side, dy, p] = value[:, p * wide : (p + 1) * wide]
                        if side == 0:
                            send(
                                part.at[k, h, 0, dy, p], r1.at[k, h, dy, p],
                                e_s.at[k, h, dy, p], e_r.at[k, h, dy, p], {"tp": mate},
                            )

        def stage_e(i, h):
            k = at(i)
            for dy in range(1, high):
                for p in range(pieces):
                    arrive(r1.at[k, h, dy, p], e_s.at[k, h, dy, p], e_r.at[k, h, dy, p])
                    s2[k, h, dy - 1, p] = (
                        part[k, h, 1, dy, p].astype(F32) + r1[k, h, dy, p].astype(F32)
                    ).astype(BF16)
                    send(
                        s2.at[k, h, dy - 1, p], r2.at[k, h, dy - 1, p],
                        g_s.at[k, h, dy - 1, p], g_r.at[k, h, dy - 1, p],
                        {"tp": up_to(dy) * CORES + cc},
                    )

        def stage_g(i, h):
            k = at(i)
            for p in range(pieces):
                arrive(r1.at[k, h, 0, p], e_s.at[k, h, 0, p], e_r.at[k, h, 0, p])
                total = part[k, h, 1, 0, p].astype(F32) + r1[k, h, 0, p].astype(F32)
                for dy in range(1, high):
                    arrive(r2.at[k, h, dy - 1, p], g_s.at[k, h, dy - 1, p], g_r.at[k, h, dy - 1, p])
                    total = total + r2[k, h, dy - 1, p].astype(F32)
                t3[k, h, p] = total.astype(BF16).reshape(size, cap, wide)
                for n, jj in enumerate(blocks(h)):
                    if is_own(i, h, n):
                        ret[p, me] = t3[k, h, p, n]
                        continue
                    dest = partner(i) * per + jj
                    send(
                        t3.at[k, h, p, n], ret.at[p, me], ret_s.at[k, h, p, n], ret_r.at[p, me],
                        {"ep": dest},
                    )

        def window_of(out, group, p, count):
            span = slab // count
            return out.at[:, pl.ds(pl.multiple_of(group * slab + p * span, span), span)]

        def spread(which, out, p, count, value):
            span = slab // count
            out[:, pl.ds(pl.multiple_of(t * slab + p * span, span), span)] = value
            window = window_of(out, t, p, count)
            for dy in range(1, high):
                send(
                    window, window, ay_s.at[which, dy - 1, p], ay_r.at[which, dy - 1, p],
                    {"tp": up_to(dy) * CORES + cc},
                )
            send(window, window, ab_s.at[which, 0, p], ab_r.at[which, 0, p], {"tp": mate})

        def spread_on(which, out, p, count):
            for dy in range(1, high):
                window = window_of(out, down_to(dy) * CORES + cc, p, count)
                arrive(window, ay_s.at[which, dy - 1, p], ay_r.at[which, dy - 1, p])
                send(window, window, ab_s.at[which, dy, p], ab_r.at[which, dy, p], {"tp": mate})

        def spread_end(which, out, p, count):
            for dy in range(high):
                arrive(
                    window_of(out, down_to(dy) * CORES + (1 - cc), p, count),
                    ab_s.at[which, dy, p], ab_r.at[which, dy, p],
                )

        def mixer_out():
            loaded("gout", "taps")
            gate_out = dot(mixed, w_gout[...])
            arrive(rim_in, rim_s.at[0], rim_r.at[0])
            first = jnp.where(me == 0, 0.0, rim_in[...].astype(F32))
            extended = jnp.concatenate([first, conv_input.astype(F32)], axis=0)
            conv = jnp.zeros((mrows, chan), F32)
            for k in range(taps_n):
                start = edge - (taps_n - 1) + k
                conv = conv + taps[k : k + 1, :] * extended[start : start + mrows]
            gated = (gate_out * conv).astype(BF16)
            loaded("mout")
            for side, core in ((0, 1 - cc), (1, cc)):
                for dy in turns:
                    m_part[side, dy] = dot(gated, w_mout[:, columns(dy, core)]).astype(BF16)
                    if side == 0:
                        send(m_part.at[0, dy], m_r1.at[dy], me_s.at[dy], me_r.at[dy], {"tp": mate})

        def mixer_pair():
            for dy in range(1, high):
                arrive(m_r1.at[dy], me_s.at[dy], me_r.at[dy])
                m_s2[dy - 1] = (m_part[1, dy].astype(F32) + m_r1[dy].astype(F32)).astype(BF16)
                send(
                    m_s2.at[dy - 1], m_r2.at[dy - 1], mg_s.at[dy - 1], mg_r.at[dy - 1],
                    {"tp": up_to(dy) * CORES + cc},
                )

        def mixer_sum():
            arrive(m_r1.at[0], me_s.at[0], me_r.at[0])
            total = m_part[1, 0].astype(F32) + m_r1[0].astype(F32)
            for dy in range(1, high):
                arrive(m_r2.at[dy - 1], mg_s.at[dy - 1], mg_r.at[dy - 1])
                total = total + m_r2[dy - 1].astype(F32)
            spread(0, out_m, 0, 1, total.astype(BF16))

        def finish(p):
            for d in range(1, experts):
                e = lax.rem(me + d, experts)
                arrive(ret.at[p, e], ret_s.at[0, 0, 0, 0], ret_r.at[p, e])
            summed = lax.dot_general(
                sum_map, ret[p].reshape(experts * cap, wide), (((0,), (0,)), ((), ())),
                preferred_element_type=F32,
            )
            spread(1, out_r, p, pieces, summed.astype(BF16))

        stages = dict(
            M=mixer_out, N=mixer_pair, O=mixer_sum, P=lambda: spread_on(0, out_m, 0, 1),
            W=lambda: loaded("gate", "up", "down"),
            A=stage_a, B=stage_b, C=stage_c, E=stage_e, G=stage_g,
        )
        for word in order:
            with jax.named_scope(word):
                stages[word[0]](*((word[1], int(word[2:])) if word[1:] else ()))
        early = sent[: 2 * len(sent) // 3]
        for copy in early:
            copy.wait_send()
        with jax.named_scope("finish"):
            for p in range(pieces):
                finish(p)
        with jax.named_scope("spreadon"):
            for p in range(pieces):
                spread_on(1, out_r, p, pieces)
        with jax.named_scope("end"):
            spread_end(0, out_m, 0, 1)
            for p in range(pieces):
                spread_end(1, out_r, p, pieces)
        for copy in sent[len(early) :]:
            copy.wait_send()

    dma = pltpu.SemaphoreType.DMA
    far = max(1, high - 1)
    v = lambda *shape: pltpu.VMEM(shape, BF16)
    f = lambda *shape: pltpu.VMEM(shape, F32)
    scratch = [
        v(mrows, width), f(1, width), f(taps_n, chan), v(tok, width), f(1, width),
        pltpu.VMEM((picks, tok), I32), f(picks, tok),
        v(width, chan), v(width, chan), v(width, chan), v(chan, width),
        v(width, hid), v(width, hid), v(hid, width),
        v(high, experts, cap, slab), v(groups, steps, per, cap, slab),
        v(steps, halves, 2, high, pieces, rows, wide), v(steps, halves, high, pieces, rows, wide),
        v(steps, halves, far, pieces, rows, wide), v(steps, halves, far, pieces, rows, wide),
        v(steps, halves, pieces, size, cap, wide), v(pieces, experts, cap, wide),
        v(edge, chan), v(edge, chan),
        v(2, high, mrows, slab), v(high, mrows, slab), v(far, mrows, slab), v(far, mrows, slab),
        dma((14,)), dma((high,)),
        dma((steps, per, high)), dma((steps, per, high)),
        dma((steps, far, per)), dma((steps, far, per)),
        dma((steps, high, per)), dma((steps, high, per)),
        dma((steps, halves, high, pieces)), dma((steps, halves, high, pieces)),
        dma((steps, halves, far, pieces)), dma((steps, halves, far, pieces)),
        dma((steps, halves, pieces, size)), dma((pieces, experts)),
        dma((1,)), dma((1,)),
        dma((high,)), dma((high,)), dma((far,)), dma((far,)),
        dma((2, far, pieces)), dma((2, far, pieces)), dma((2, high, pieces)), dma((2, high, pieces)),
    ]
    return kernel, scratch


def store(a, b, out_a, out_b, sem):
    copies = [
        pltpu.make_async_copy(a, out_a, sem.at[0]), pltpu.make_async_copy(b, out_b, sem.at[1])
    ]
    for copy in copies:
        copy.start()
    for copy in copies:
        copy.wait()


def on_device(
    mixer_rows, mixer_gain, inner_weight, gate_in_weight, gate_out_weight, conv_taps,
    mixer_out_weight, routed_rows, routed_gain, route_ids, route_weights,
    expert_gate, expert_up, expert_down,
):
    experts, groups = lax.axis_size("ep"), lax.axis_size("tp")
    tok, picks = route_ids.shape
    width = routed_rows.shape[1]
    cap = 2 * tok * picks // experts
    per = max(1, min(experts, tok // cap))
    steps = experts // per
    mrows = mixer_rows.shape[0]
    taps_n, chan = conv_taps.shape
    whole = 2 if groups // CORES == 2 else 1
    pieces = max(1, min(2, width // groups // 256))
    kernel, scratch = make_kernel(
        experts, groups, tok, picks, width, cap, steps, per, mrows, taps_n, chan,
        expert_gate.shape[2], whole, *schedule(steps, per, whole), pieces,
    )
    near, far = pl.BlockSpec(memory_space=pltpu.VMEM), pl.BlockSpec(memory_space=pl.ANY)
    done = pl.pallas_call(
        kernel,
        out_shape=(pltpu.VMEM(mixer_rows.shape, BF16), pltpu.VMEM(routed_rows.shape, BF16)),
        in_specs=[far] * 14,
        out_specs=(near, near),
        scratch_shapes=scratch,
        compiler_params=pltpu.CompilerParams(
            collective_id=0, has_side_effects=True, vmem_limit_bytes=60 * 1024 * 1024
        ),
        name="mixer_and_experts",
    )(
        mixer_rows, mixer_gain[None, :], inner_weight, gate_in_weight, gate_out_weight, conv_taps,
        mixer_out_weight, routed_rows, routed_gain[None, :], route_ids.T, route_weights.T,
        expert_gate[0], expert_up[0], expert_down[0],
    )
    return pl.pallas_call(
        store,
        out_shape=(
            jax.ShapeDtypeStruct(mixer_rows.shape, BF16),
            jax.ShapeDtypeStruct(routed_rows.shape, BF16),
        ),
        in_specs=[far, far],
        out_specs=(far, far),
        scratch_shapes=[pltpu.SemaphoreType.DMA((2,))],
        name="store",
    )(*(pltpu.with_memory_space_constraint(array, pltpu.VMEM) for array in done))


def solution(mesh):
    return jax.shard_map(
        on_device,
        mesh=mesh,
        in_specs=(
            P("ep", None), P(), P(None, "tp"), P(None, "tp"), P(None, "tp"), P(None, "tp"),
            P("tp", None), P("ep", None), P(), P("ep", None), P("ep", None),
            P("ep", None, "tp"), P("ep", None, "tp"), P("ep", "tp", None),
        ),
        out_specs=(P("ep", None), P("ep", None)),
        check_vma=False,
    )
```

time: 97.1 us -> 73 us (0.75)
  the two profiles are of different devices: /device:TPU:0 before, /device:TPU:31 now
where the time goes in v1:
time: 73 us; the launch traced here: 72.8 us
  Pallas kernels  72.1 us (99%)
    pallas_call x1, Pallas kernels, on_device(): pl.pallas_call(kernel, out_shape=(pltpu.VMEM(mixer_rows.shape, BF16), plt...  71 us

profile of v1, /device:TPU:31, one launch (start us, length us, event | category | flops | bytes accessed | tf_op | source)
XLA Modules:
  0.0 72.8 jit_solution(2587182237264745490)
XLA Ops:
  0.6 71.0 %mixer_and_experts.1 = (bf16[128,2048]{1,0:T(8,128)(2,1)S(1)}, bf16[256,2048]{1,0:T(8,128)(2,1)S(1)}) custom-call(bf16[128,2048]{1,0:T(8,128)(2,1)} %mixer_h.1, f32[1,2048]{1,0:T(1,128)} %bitcast.10, bf16[2048,256]{1,0:T(8,128)(2,1)} %inner_h.1, bf16[2048,256]{1,0:T(8,128)(2,1)} %gate_in_h.1, bf16[2048,256]{1,0:T(8,128)(2,1)} %gate_out_h.1, ...), custom_call_target="tpu_custom_call" | custom-call | tf_op jit(solution)/shard_map/mixer_and_experts/pallas_call | solution.py:465
  71.6 1.2 %store.1 = (bf16[128,2048]{1,0:T(8,128)(2,1)}, bf16[256,2048]{1,0:T(8,128)(2,1)}) custom-call(bf16[128,2048]{1,0:T(8,128)(2,1)S(1)} %get-tuple-element.4.a, bf16[256,2048]{1,0:T(8,128)(2,1)S(1)} %get-tuple-element.5.b), custom_call_target="tpu_custom_call" | custom-call | tf_op jit(solution)/shard_map/store/pallas_call | solution.py:480

commit v2 on v1

--- a/solution.py
+++ b/solution.py
@@ -19,18 +19,20 @@
 
 ORDER = (
     "W", "C00", "E00", "M", "N", "A01", "Aa0", "O", "C01", "E01",
-    "Aa1", "Ba0", "Ca0", "Ea0", "A10", "Ab0", "P", "Ba1", "Ca1", "Ea1",
-    "G00", "G01", "Ga0", "Ab1", "A11", "Bb0", "Cb0", "Eb0", "Ga1", "C10",
-    "E10", "Bb1", "Cb1", "Gb0", "Eb1", "C11", "E11", "Gb1", "G10", "G11",
+    "T", "Aa1", "Ba0", "Ca0", "Ea0", "A10", "Ab0", "P", "Ba1", "Ca1",
+    "Ea1", "G00", "G01", "Ga0", "Ab1", "A11", "Bb0", "Cb0", "Eb0", "Ga1",
+    "C10", "E10", "Bb1", "Cb1", "Gb00", "Eb1", "C11", "E11", "Gb10", "G100",
+    "Gb01", "Gb11", "G110", "G101", "G111",
 )
 QUEUE = ("01", "20", "30", "21", "31", "10", "11")
+KINDS = ("d1", "y", "b", "e", "g", "ret", "rim", "me", "mg", "ay", "ab")
 
 
 def schedule(steps, per, whole):
     if steps == 4 and per == 2 and whole == 2:
         return 2, QUEUE, ORDER
     queue = [str(i) for i in range(steps)]
-    order = ["M", "N", "W", "A00", "C00", "O", "E00", "P"]
+    order = ["M", "N", "T", "W", "A00", "C00", "O", "E00", "P"]
     for last, i in zip(queue, queue[1:]):
         order += [name + i + "0" for name in ("AC" if int(i) < whole else "ABC") + "E"]
         order.append("G" + last + "0")
@@ -54,29 +56,58 @@
         mixer_rows, mixer_gain, taps, routed_rows, routed_gain, ids, weights,
         w_inner, w_gin, w_gout, w_mout, w_gate, w_up, w_down,
         disp, slots, part, r1, s2, r2, t3, ret,
+        sums,
         rim, rim_in, m_part, m_r1, m_s2, m_r2,
-        w_sem, own_sem,
-        d1_s, d1_r, y_s, y_r, b_s, b_r, e_s, e_r, g_s, g_r, ret_s, ret_r,
-        rim_s, rim_r, me_s, me_r, mg_s, mg_r, ay_s, ay_r, ab_s, ab_r,
+        w_sem, own_sem, s_sem,
+        d1_r, y_r, b_r, e_r, g_r, ret_r,
+        rim_r, me_r, mg_r, ay_r, ab_r,
     ):
         me = lax.axis_index("ep")
         t = lax.axis_index("tp")
         yy, cc = t // CORES, t % CORES
         mate = yy * CORES + (1 - cc)
         my_chunk, my_j = me // per, me % per
-        sent = []
-
-        def send(src, dst, ssem, rsem, where):
+        sent = {}
+
+        def send(src, dst, kind, rsem, where):
             copy = pltpu.make_async_remote_copy(
-                src_ref=src, dst_ref=dst, send_sem=ssem, recv_sem=rsem,
+                src_ref=src, dst_ref=dst, send_sem=s_sem.at[KINDS.index(kind)], recv_sem=rsem,
                 device_id=where, device_id_type=pl.DeviceIdType.MESH,
             )
             copy.start()
-            sent.append(copy)
-
-        def arrive(dst, ssem, rsem):
+            sent[kind] = sent.get(kind, 0) + volume(src.shape)
+
+        def volume(shape):
+            total = 1
+            for n in shape:
+                total *= n
+            return total
+
+        def carrier(count):
+            for ref in (gate_h, disp, slots, part):
+                line = volume(ref.shape[1:])
+                if count % line == 0 and count // line <= ref.shape[0]:
+                    return ref.at[0 : count // line]
+            for ref in (disp, slots):
+                for a in range(1, ref.shape[0] + 1):
+                    line = a * volume(ref.shape[2:])
+                    if count % line == 0 and count // line <= ref.shape[1]:
+                        return ref.at[0:a, 0 : count // line]
+            raise ValueError(count)
+
+        def drain(*kinds):
+            for kind in kinds:
+                if kind in sent:
+                    ref = carrier(sent.pop(kind))
+                    pltpu.make_async_remote_copy(
+                        src_ref=ref, dst_ref=ref, send_sem=s_sem.at[KINDS.index(kind)],
+                        recv_sem=s_sem.at[KINDS.index(kind)],
+                        device_id={"tp": mate}, device_id_type=pl.DeviceIdType.MESH,
+                    ).wait_send()
+
+        def arrive(dst, rsem):
             pltpu.make_async_remote_copy(
-                src_ref=dst, dst_ref=dst, send_sem=ssem, recv_sem=rsem,
+                src_ref=dst, dst_ref=dst, send_sem=s_sem.at[0], recv_sem=rsem,
                 device_id={"tp": mate}, device_id_type=pl.DeviceIdType.MESH,
             ).wait_recv()
 
@@ -130,13 +161,19 @@
             earlier = dot(named.astype(BF16), before)
             slot_row = lax.broadcasted_iota(I32, (experts * cap, tok), 0)
             pick_map = jnp.zeros((experts * cap, tok), F32)
-            sum_map = jnp.zeros((experts * cap, tok), F32)
+            placed = []
             for k in range(picks):
                 rank = jnp.sum(jnp.where(hits[k], earlier, 0.0), axis=0, keepdims=True).astype(I32)
-                at = slot_row == (ids[k : k + 1, :] * cap + rank)
-                pick_map = pick_map + jnp.where(at, 1.0, 0.0)
-                sum_map = sum_map + jnp.where(at, weights[k : k + 1, :], 0.0)
-            pick_map, sum_map = pick_map.astype(BF16), sum_map.astype(BF16)
+                placed.append(ids[k : k + 1, :] * cap + rank)
+                pick_map = pick_map + jnp.where(slot_row == placed[k], 1.0, 0.0)
+            pick_map = pick_map.astype(BF16)
+
+        def weigh():
+            slot_row = lax.broadcasted_iota(I32, (experts * cap, tok), 0)
+            total = jnp.zeros((experts * cap, tok), F32)
+            for k in range(picks):
+                total = total + jnp.where(slot_row == placed[k], weights[k : k + 1, :], 0.0)
+            sums[...] = total.T.astype(BF16)
 
         my_cols = pl.ds(pl.multiple_of(t * slab, slab), slab)
 
@@ -160,7 +197,7 @@
 
         with jax.named_scope("barrier"):
             pl.semaphore_wait(barrier, experts - 1 + high - 1 + 1)
-        send(rim, rim_in, rim_s.at[0], rim_r.at[0], {"ep": lax.rem(me + 1, experts)})
+        send(rim, rim_in, "rim", rim_r.at[0], {"ep": lax.rem(me + 1, experts)})
 
         def blocks(h):
             return [lax.rem(my_j + h * size + n, per) for n in range(size)]
@@ -191,16 +228,13 @@
                 if not is_own(i, h, n):
                     dest = partner(i) * per + jj
                     for dy in slabs(i):
-                        send(
-                            disp.at[dy, dest], slots.at[down_to(dy) * CORES + cc, at(i), my_j],
-                            d1_s.at[at(i), jj, dy], d1_r.at[at(i), my_j, dy], {"ep": dest},
-                        )
+                        send(disp.at[dy, dest], slots.at[down_to(dy) * CORES + cc, at(i), my_j], "d1", d1_r.at[at(i), my_j], {"ep": dest})
 
         own = []
 
         def keep(dy):
             block = slots.at[down_to(dy) * CORES + cc, 0, my_j]
-            send(disp.at[dy, me], block, b_s.at[0, dy, my_j], b_r.at[0, dy, my_j], {"tp": mate})
+            send(disp.at[dy, me], block, "b", b_r.at[0, 0], {"tp": mate})
             copy = pltpu.make_async_copy(disp.at[dy, me], block, own_sem.at[dy])
             copy.start()
             own.append(copy)
@@ -218,24 +252,23 @@
             for n, jj in enumerate(blocks(h)):
                 if is_own(i, h, n):
                     continue
+                arrive(slots.at[0 : len(slabs(i)), k, jj], d1_r.at[k, jj])
                 for dy in slabs(i):
                     block = slots.at[down_to(dy) * CORES + cc, k, jj]
-                    arrive(block, d1_s.at[k, jj, dy], d1_r.at[k, jj, dy])
                     if far(i):
                         for up in range(1, high):
                             send(
-                                block, block, y_s.at[k, up - 1, jj], y_r.at[k, up - 1, jj],
-                                {"tp": up_to(up) * CORES + cc},
+                                block, block, "y", y_r.at[k, up - 1, jj], {"tp": up_to(up) * CORES + cc}
                             )
-                    send(block, block, b_s.at[k, dy, jj], b_r.at[k, dy, jj], {"tp": mate})
+                    send(block, block, "b", b_r.at[k, h], {"tp": mate})
 
         def stage_b(i, h):
             k = at(i)
             for dy in range(1, high):
                 for jj in blocks(h):
                     block = slots.at[down_to(dy) * CORES + cc, k, jj]
-                    arrive(block, y_s.at[k, dy - 1, jj], y_r.at[k, dy - 1, jj])
-                    send(block, block, b_s.at[k, dy, jj], b_r.at[k, dy, jj], {"tp": mate})
+                    arrive(block, y_r.at[k, dy - 1, jj])
+                    send(block, block, "b", b_r.at[k, h], {"tp": mate})
 
         turns = list(range(1, high)) + [0]
 
@@ -244,12 +277,7 @@
 
         def stage_c(i, h):
             k = at(i)
-            for dy in range(high):
-                for jj in blocks(h):
-                    arrive(
-                        slots.at[down_to(dy) * CORES + (1 - cc), k, jj],
-                        b_s.at[k, dy, jj], b_r.at[k, dy, jj],
-                    )
+            arrive(slots.at[0:high, k, 0:size], b_r.at[k, h])
             if is_own(i, h, 0):
                 for copy in own:
                     copy.wait()
@@ -267,33 +295,30 @@
                     value = dot(hidden, w_down[:, columns(dy, core)]).astype(BF16)
                     for p in range(pieces):
                         part[k, h, side, dy, p] = value[:, p * wide : (p + 1) * wide]
-                        if side == 0:
-                            send(
-                                part.at[k, h, 0, dy, p], r1.at[k, h, dy, p],
-                                e_s.at[k, h, dy, p], e_r.at[k, h, dy, p], {"tp": mate},
-                            )
+                    if side == 0:
+                        send(part.at[k, h, 0, dy], r1.at[k, h, dy], "e", e_r.at[k, h, dy], {"tp": mate})
 
         def stage_e(i, h):
             k = at(i)
             for dy in range(1, high):
+                arrive(r1.at[k, h, dy], e_r.at[k, h, dy])
                 for p in range(pieces):
-                    arrive(r1.at[k, h, dy, p], e_s.at[k, h, dy, p], e_r.at[k, h, dy, p])
                     s2[k, h, dy - 1, p] = (
                         part[k, h, 1, dy, p].astype(F32) + r1[k, h, dy, p].astype(F32)
                     ).astype(BF16)
                     send(
-                        s2.at[k, h, dy - 1, p], r2.at[k, h, dy - 1, p],
-                        g_s.at[k, h, dy - 1, p], g_r.at[k, h, dy - 1, p],
+                        s2.at[k, h, dy - 1, p], r2.at[k, h, dy - 1, p], "g", g_r.at[k, h, dy - 1, p],
                         {"tp": up_to(dy) * CORES + cc},
                     )
 
-        def stage_g(i, h):
+        def stage_g(i, h, *only):
             k = at(i)
-            for p in range(pieces):
-                arrive(r1.at[k, h, 0, p], e_s.at[k, h, 0, p], e_r.at[k, h, 0, p])
+            for p in only or range(pieces):
+                if p == 0:
+                    arrive(r1.at[k, h, 0], e_r.at[k, h, 0])
                 total = part[k, h, 1, 0, p].astype(F32) + r1[k, h, 0, p].astype(F32)
                 for dy in range(1, high):
-                    arrive(r2.at[k, h, dy - 1, p], g_s.at[k, h, dy - 1, p], g_r.at[k, h, dy - 1, p])
+                    arrive(r2.at[k, h, dy - 1, p], g_r.at[k, h, dy - 1, p])
                     total = total + r2[k, h, dy - 1, p].astype(F32)
                 t3[k, h, p] = total.astype(BF16).reshape(size, cap, wide)
                 for n, jj in enumerate(blocks(h)):
@@ -301,10 +326,7 @@
                         ret[p, me] = t3[k, h, p, n]
                         continue
                     dest = partner(i) * per + jj
-                    send(
-                        t3.at[k, h, p, n], ret.at[p, me], ret_s.at[k, h, p, n], ret_r.at[p, me],
-                        {"ep": dest},
-                    )
+                    send(t3.at[k, h, p, n], ret.at[p, me], "ret", ret_r.at[p], {"ep": dest})
 
         def window_of(out, group, p, count):
             span = slab // count
@@ -315,29 +337,22 @@
             out[:, pl.ds(pl.multiple_of(t * slab + p * span, span), span)] = value
             window = window_of(out, t, p, count)
             for dy in range(1, high):
-                send(
-                    window, window, ay_s.at[which, dy - 1, p], ay_r.at[which, dy - 1, p],
-                    {"tp": up_to(dy) * CORES + cc},
-                )
-            send(window, window, ab_s.at[which, 0, p], ab_r.at[which, 0, p], {"tp": mate})
+                send(window, window, "ay", ay_r.at[which, dy - 1, p], {"tp": up_to(dy) * CORES + cc})
+            send(window, window, "ab", ab_r.at[which], {"tp": mate})
 
         def spread_on(which, out, p, count):
             for dy in range(1, high):
                 window = window_of(out, down_to(dy) * CORES + cc, p, count)
-                arrive(window, ay_s.at[which, dy - 1, p], ay_r.at[which, dy - 1, p])
-                send(window, window, ab_s.at[which, dy, p], ab_r.at[which, dy, p], {"tp": mate})
-
-        def spread_end(which, out, p, count):
-            for dy in range(high):
-                arrive(
-                    window_of(out, down_to(dy) * CORES + (1 - cc), p, count),
-                    ab_s.at[which, dy, p], ab_r.at[which, dy, p],
-                )
+                arrive(window, ay_r.at[which, dy - 1, p])
+                send(window, window, "ab", ab_r.at[which], {"tp": mate})
+
+        def spread_end(which, out):
+            arrive(out.at[:, pl.ds(0, high * slab)], ab_r.at[which])
 
         def mixer_out():
             loaded("gout", "taps")
             gate_out = dot(mixed, w_gout[...])
-            arrive(rim_in, rim_s.at[0], rim_r.at[0])
+            arrive(rim_in, rim_r.at[0])
             first = jnp.where(me == 0, 0.0, rim_in[...].astype(F32))
             extended = jnp.concatenate([first, conv_input.astype(F32)], axis=0)
             conv = jnp.zeros((mrows, chan), F32)
@@ -350,58 +365,49 @@
                 for dy in turns:
                     m_part[side, dy] = dot(gated, w_mout[:, columns(dy, core)]).astype(BF16)
                     if side == 0:
-                        send(m_part.at[0, dy], m_r1.at[dy], me_s.at[dy], me_r.at[dy], {"tp": mate})
+                        send(m_part.at[0, dy], m_r1.at[dy], "me", me_r.at[dy], {"tp": mate})
 
         def mixer_pair():
             for dy in range(1, high):
-                arrive(m_r1.at[dy], me_s.at[dy], me_r.at[dy])
+                arrive(m_r1.at[dy], me_r.at[dy])
                 m_s2[dy - 1] = (m_part[1, dy].astype(F32) + m_r1[dy].astype(F32)).astype(BF16)
-                send(
-                    m_s2.at[dy - 1], m_r2.at[dy - 1], mg_s.at[dy - 1], mg_r.at[dy - 1],
-                    {"tp": up_to(dy) * CORES + cc},
-                )
+                send(m_s2.at[dy - 1], m_r2.at[dy - 1], "mg", mg_r.at[dy - 1], {"tp": up_to(dy) * CORES + cc})
 
         def mixer_sum():
-            arrive(m_r1.at[0], me_s.at[0], me_r.at[0])
+            arrive(m_r1.at[0], me_r.at[0])
             total = m_part[1, 0].astype(F32) + m_r1[0].astype(F32)
             for dy in range(1, high):
-                arrive(m_r2.at[dy - 1], mg_s.at[dy - 1], mg_r.at[dy - 1])
+                arrive(m_r2.at[dy - 1], mg_r.at[dy - 1])
                 total = total + m_r2[dy - 1].astype(F32)
             spread(0, out_m, 0, 1, total.astype(BF16))
 
         def finish(p):
-            for d in range(1, experts):
-                e = lax.rem(me + d, experts)
-                arrive(ret.at[p, e], ret_s.at[0, 0, 0, 0], ret_r.at[p, e])
-            summed = lax.dot_general(
-                sum_map, ret[p].reshape(experts * cap, wide), (((0,), (0,)), ((), ())),
-                preferred_element_type=F32,
-            )
-            spread(1, out_r, p, pieces, summed.astype(BF16))
+            arrive(ret.at[p, 0 : experts - 1], ret_r.at[p])
+            total = dot(sums[...], ret[p].reshape(experts * cap, wide))
+            spread(1, out_r, p, pieces, total.astype(BF16))
 
         stages = dict(
             M=mixer_out, N=mixer_pair, O=mixer_sum, P=lambda: spread_on(0, out_m, 0, 1),
-            W=lambda: loaded("gate", "up", "down"),
+            W=lambda: loaded("gate", "up", "down"), T=weigh,
             A=stage_a, B=stage_b, C=stage_c, E=stage_e, G=stage_g,
         )
         for word in order:
             with jax.named_scope(word):
-                stages[word[0]](*((word[1], int(word[2:])) if word[1:] else ()))
-        early = sent[: 2 * len(sent) // 3]
-        for copy in early:
-            copy.wait_send()
-        with jax.named_scope("finish"):
-            for p in range(pieces):
+                stages[word[0]](*((word[1], *(int(c) for c in word[2:])) if word[1:] else ()))
+        with jax.named_scope("early"):
+            drain("d1", "y", "b", "e", "rim", "me", "mg")
+        for p in range(pieces):
+            with jax.named_scope("finish%d" % p):
                 finish(p)
         with jax.named_scope("spreadon"):
+            drain("g", "ret")
             for p in range(pieces):
                 spread_on(1, out_r, p, pieces)
         with jax.named_scope("end"):
-            spread_end(0, out_m, 0, 1)
-            for p in range(pieces):
-                spread_end(1, out_r, p, pieces)
-        for copy in sent[len(early) :]:
-            copy.wait_send()
+            spread_end(0, out_m)
+            spread_end(1, out_r)
+        with jax.named_scope("drain"):
+            drain("ay", "ab")
 
     dma = pltpu.SemaphoreType.DMA
     far = max(1, high - 1)
@@ -416,18 +422,13 @@
         v(steps, halves, 2, high, pieces, rows, wide), v(steps, halves, high, pieces, rows, wide),
         v(steps, halves, far, pieces, rows, wide), v(steps, halves, far, pieces, rows, wide),
         v(steps, halves, pieces, size, cap, wide), v(pieces, experts, cap, wide),
+        v(tok, experts * cap),
         v(edge, chan), v(edge, chan),
         v(2, high, mrows, slab), v(high, mrows, slab), v(far, mrows, slab), v(far, mrows, slab),
-        dma((14,)), dma((high,)),
-        dma((steps, per, high)), dma((steps, per, high)),
-        dma((steps, far, per)), dma((steps, far, per)),
-        dma((steps, high, per)), dma((steps, high, per)),
-        dma((steps, halves, high, pieces)), dma((steps, halves, high, pieces)),
-        dma((steps, halves, far, pieces)), dma((steps, halves, far, pieces)),
-        dma((steps, halves, pieces, size)), dma((pieces, experts)),
-        dma((1,)), dma((1,)),
-        dma((high,)), dma((high,)), dma((far,)), dma((far,)),
-        dma((2, far, pieces)), dma((2, far, pieces)), dma((2, high, pieces)), dma((2, high, pieces)),
+        dma((14,)), dma((high,)), dma((len(KINDS),)),
+        dma((steps, per)), dma((steps, far, per)), dma((steps, halves)),
+        dma((steps, halves, high)), dma((steps, halves, far, pieces)), dma((pieces,)),
+        dma((1,)), dma((high,)), dma((far,)), dma((2, far, pieces)), dma((2,)),
     ]
     return kernel, scratch
 

time: 73 us -> 70 us (0.959)
  Pallas kernels: 72.1 us -> 69.2 us
    pallas_call x1, Pallas kernels: 71 us -> 68 us  [on_device(): pl.pallas_call(kernel, out_shape=(pltpu.VMEM(mixer_rows.shape, BF16), plt...]
where the time goes in v2:
time: 70 us; the launch traced here: 69.9 us
  Pallas kernels  69.2 us (99%)
    pallas_call x1, Pallas kernels, on_device(): pl.pallas_call(kernel, out_shape=(pltpu.VMEM(mixer_rows.shape, BF16), plt...  68 us

profile of v2, /device:TPU:31, one launch (start us, length us, event | category | flops | bytes accessed | tf_op | source)
XLA Modules:
  0.0 69.9 jit_solution(11742207069270764842)
XLA Ops:
  0.6 68.0 %mixer_and_experts.1 = (bf16[128,2048]{1,0:T(8,128)(2,1)S(1)}, bf16[256,2048]{1,0:T(8,128)(2,1)S(1)}) custom-call(bf16[128,2048]{1,0:T(8,128)(2,1)} %mixer_h.1, f32[1,2048]{1,0:T(1,128)} %bitcast.10, bf16[2048,256]{1,0:T(8,128)(2,1)} %inner_h.1, bf16[2048,256]{1,0:T(8,128)(2,1)} %gate_in_h.1, bf16[2048,256]{1,0:T(8,128)(2,1)} %gate_out_h.1, ...), custom_call_target="tpu_custom_call" | custom-call | tf_op jit(solution)/shard_map/mixer_and_experts/pallas_call | solution.py:466
  68.7 1.2 %store.1 = (bf16[128,2048]{1,0:T(8,128)(2,1)}, bf16[256,2048]{1,0:T(8,128)(2,1)}) custom-call(bf16[128,2048]{1,0:T(8,128)(2,1)S(1)} %get-tuple-element.4.a, bf16[256,2048]{1,0:T(8,128)(2,1)S(1)} %get-tuple-element.5.b), custom_call_target="tpu_custom_call" | custom-call | tf_op jit(solution)/shard_map/store/pallas_call | solution.py:481

commit v3 on v2

--- a/solution.py
+++ b/solution.py
@@ -17,13 +17,7 @@
     return jnp.dot(a, b, preferred_element_type=F32)
 
 
-ORDER = (
-    "W", "C00", "E00", "M", "N", "A01", "Aa0", "O", "C01", "E01",
-    "T", "Aa1", "Ba0", "Ca0", "Ea0", "A10", "Ab0", "P", "Ba1", "Ca1",
-    "Ea1", "G00", "G01", "Ga0", "Ab1", "A11", "Bb0", "Cb0", "Eb0", "Ga1",
-    "C10", "E10", "Bb1", "Cb1", "Gb00", "Eb1", "C11", "E11", "Gb10", "G100",
-    "Gb01", "Gb11", "G110", "G101", "G111",
-)
+ORDER = ("W", "C00", "E00", "M", "N", "A01", "Aa0", "O", "C01", "T", "Aa1", "Ba0", "Ca0", "Ea0", "A10", "Ab0", "P", "Ba1", "Ca1", "Ga0", "Ea1", "E01", "G00", "Ab1", "A11", "Bb0", "Cb0", "Eb0", "Ga1", "C10", "E10", "Bb1", "Cb1", "Gb00", "Eb1", "C11", "E11", "G01", "Gb10", "G100", "Gb01", "Gb11", "G110", "G101", "G111", "Gb02", "Gb12", "G102", "G112", "Gb03", "Gb13", "G103", "G113")
 QUEUE = ("01", "20", "30", "21", "31", "10", "11")
 KINDS = ("d1", "y", "b", "e", "g", "ret", "rim", "me", "mg", "ay", "ab")
 
@@ -184,20 +178,23 @@
             conv_input = (dot(mixed, w_gin[...]) * dot(mixed, w_inner[...])).astype(BF16)
             rim[...] = conv_input[mrows - edge :]
 
-        def pick(dy, scale):
+        def normed(dy, scale):
             y = down_to(dy)
             cols = pl.ds(pl.multiple_of((y * CORES + cc) * slab, slab), slab)
-            normed = ((routed_rows[:, cols].astype(F32) * scale) * routed_gain[:, cols]).astype(BF16)
-            disp[dy] = dot(pick_map, normed).astype(BF16).reshape(experts, cap, slab)
+            return ((routed_rows[:, cols].astype(F32) * scale) * routed_gain[:, cols]).astype(BF16)
+
+        def pick(dy):
+            disp[dy] = dot(pick_map, rows_of[dy]).astype(BF16).reshape(experts, cap, slab)
 
         with jax.named_scope("pick"):
             loaded("routed", "rgain")
             scale = rms(routed_rows[...].astype(F32))
-            pick(0, scale)
+            rows_of = [normed(dy, scale) for dy in range(high)]
 
         with jax.named_scope("barrier"):
             pl.semaphore_wait(barrier, experts - 1 + high - 1 + 1)
         send(rim, rim_in, "rim", rim_r.at[0], {"ep": lax.rem(me + 1, experts)})
+        pick(0)
 
         def blocks(h):
             return [lax.rem(my_j + h * size + n, per) for n in range(size)]
@@ -242,7 +239,7 @@
         with jax.named_scope("dispatch"):
             keep(0)
             for dy in range(1, high):
-                pick(dy, scale)
+                pick(dy)
                 keep(dy)
             for word in queue:
                 dispatch(word[0], int(word[1]))
@@ -457,7 +454,7 @@
     mrows = mixer_rows.shape[0]
     taps_n, chan = conv_taps.shape
     whole = 2 if groups // CORES == 2 else 1
-    pieces = max(1, min(2, width // groups // 256))
+    pieces = max(1, min(4, width // groups // 128))
     kernel, scratch = make_kernel(
         experts, groups, tok, picks, width, cap, steps, per, mrows, taps_n, chan,
         expert_gate.shape[2], whole, *schedule(steps, per, whole), pieces,

time: 70 us -> 67.3 us (0.961)
  the two profiles are of different devices: /device:TPU:31 before, /device:TPU:9 now
where the time goes in v3:
time: 67.3 us; the launch traced here: 67.1 us
  Pallas kernels  66.5 us (99%)
    pallas_call x1, Pallas kernels, on_device(): pl.pallas_call(kernel, out_shape=(pltpu.VMEM(mixer_rows.shape, BF16), plt...  65.3 us

profile of v3, /device:TPU:9, one launch (start us, length us, event | category | flops | bytes accessed | tf_op | source)
XLA Modules:
  0.0 67.1 jit_solution(14178176065371605102)
XLA Ops:
  0.6 65.3 %mixer_and_experts.1 = (bf16[128,2048]{1,0:T(8,128)(2,1)S(1)}, bf16[256,2048]{1,0:T(8,128)(2,1)S(1)}) custom-call(bf16[128,2048]{1,0:T(8,128)(2,1)} %mixer_h.1, f32[1,2048]{1,0:T(1,128)} %bitcast.10, bf16[2048,256]{1,0:T(8,128)(2,1)} %inner_h.1, bf16[2048,256]{1,0:T(8,128)(2,1)} %gate_in_h.1, bf16[2048,256]{1,0:T(8,128)(2,1)} %gate_out_h.1, ...), custom_call_target="tpu_custom_call" | custom-call | tf_op jit(solution)/shard_map/mixer_and_experts/pallas_call | solution.py:463
  66.0 1.2 %store.1 = (bf16[128,2048]{1,0:T(8,128)(2,1)}, bf16[256,2048]{1,0:T(8,128)(2,1)}) custom-call(bf16[128,2048]{1,0:T(8,128)(2,1)S(1)} %get-tuple-element.4.a, bf16[256,2048]{1,0:T(8,128)(2,1)S(1)} %get-tuple-element.5.b), custom_call_target="tpu_custom_call" | custom-call | tf_op jit(solution)/shard_map/store/pallas_call | solution.py:478

commit v4 on v3

--- a/solution.py
+++ b/solution.py
@@ -17,7 +17,14 @@
     return jnp.dot(a, b, preferred_element_type=F32)
 
 
-ORDER = ("W", "C00", "E00", "M", "N", "A01", "Aa0", "O", "C01", "T", "Aa1", "Ba0", "Ca0", "Ea0", "A10", "Ab0", "P", "Ba1", "Ca1", "Ga0", "Ea1", "E01", "G00", "Ab1", "A11", "Bb0", "Cb0", "Eb0", "Ga1", "C10", "E10", "Bb1", "Cb1", "Gb00", "Eb1", "C11", "E11", "G01", "Gb10", "G100", "Gb01", "Gb11", "G110", "G101", "G111", "Gb02", "Gb12", "G102", "G112", "Gb03", "Gb13", "G103", "G113")
+ORDER = (
+    "W", "C00", "E00", "M", "N", "A01", "Aa0", "C01", "O", "T",
+    "Ba0", "Aa1", "Ca0", "Ea0", "A10", "Ba1", "Ab0", "P", "Ca1", "Ga0",
+    "Ea1", "E01", "G00", "Bb0", "Ab1", "A11", "Cb0", "Ga1", "Eb0", "C10",
+    "Bb1", "E10", "Cb1", "Gb00", "Gb01", "Eb1", "C11", "E11", "G01", "Gb10",
+    "G100", "Gb11", "G110", "Gb02", "G101", "G111", "Gb12", "G102", "G112", "Gb03",
+    "Gb13", "G103", "G113",
+)
 QUEUE = ("01", "20", "30", "21", "31", "10", "11")
 KINDS = ("d1", "y", "b", "e", "g", "ret", "rim", "me", "mg", "ay", "ab")
 

time: 67.3 us -> 66.1 us (0.982)
  Pallas kernels: 66.5 us -> 65.3 us
    pallas_call x1, Pallas kernels: 65.3 us -> 64.1 us  [on_device(): pl.pallas_call(kernel, out_shape=(pltpu.VMEM(mixer_rows.shape, BF16), plt...]
where the time goes in v4:
time: 66.1 us; the launch traced here: 65.9 us
  Pallas kernels  65.3 us (99%)
    pallas_call x1, Pallas kernels, on_device(): pl.pallas_call(kernel, out_shape=(pltpu.VMEM(mixer_rows.shape, BF16), plt...  64.1 us

profile of v4, /device:TPU:9, one launch (start us, length us, event | category | flops | bytes accessed | tf_op | source)
XLA Modules:
  0.0 65.9 jit_solution(6478795949320178657)
XLA Ops:
  0.6 64.1 %mixer_and_experts.1 = (bf16[128,2048]{1,0:T(8,128)(2,1)S(1)}, bf16[256,2048]{1,0:T(8,128)(2,1)S(1)}) custom-call(bf16[128,2048]{1,0:T(8,128)(2,1)} %mixer_h.1, f32[1,2048]{1,0:T(1,128)} %bitcast.10, bf16[2048,256]{1,0:T(8,128)(2,1)} %inner_h.1, bf16[2048,256]{1,0:T(8,128)(2,1)} %gate_in_h.1, bf16[2048,256]{1,0:T(8,128)(2,1)} %gate_out_h.1, ...), custom_call_target="tpu_custom_call" | custom-call | tf_op jit(solution)/shard_map/mixer_and_experts/pallas_call | solution.py:470
  64.8 1.2 %store.1 = (bf16[128,2048]{1,0:T(8,128)(2,1)}, bf16[256,2048]{1,0:T(8,128)(2,1)}) custom-call(bf16[128,2048]{1,0:T(8,128)(2,1)S(1)} %get-tuple-element.4.a, bf16[256,2048]{1,0:T(8,128)(2,1)S(1)} %get-tuple-element.5.b), custom_call_target="tpu_custom_call" | custom-call | tf_op jit(solution)/shard_map/store/pallas_call | solution.py:485
